TPU v7x, 256 devices: a whole 4x4x8 slice. The times are simulated.
256 devices in a mesh: sp: 64 (over z, x, core), tp: 4 (over y).
Axes of the slice: x: 4, y: 4, z: 8, core: 2. Of those that a mesh axis runs over, the one named last changes fastest.
Arguments:
- residual: bfloat16 [16384, 2048], P(('sp', 'tp')), may hold values from -6 to 6
- query_wide: bfloat16 [16384, 512], P('sp', 'tp'), may hold values from -8 to 8
- key_wide: bfloat16 [16384, 512], P('sp', 'tp'), may hold values from -8 to 8
- value_wide: bfloat16 [16384, 512], P('sp', 'tp'), may hold values from -6 to 6
- query_narrow: bfloat16 [16384, 512], P('sp', 'tp'), may hold values from -8 to 8
- key_narrow: bfloat16 [16384, 512], P('sp', 'tp'), may hold values from -8 to 8
- value_narrow: bfloat16 [16384, 512], P('sp', 'tp'), may hold values from -6 to 6
- gate_wide: float32 [16384, 4], P('sp', 'tp'), may hold values from -2 to 20
- gate_narrow: float32 [16384, 8], P('sp', 'tp'), may hold values from -2 to 20
- out_wide: bfloat16 [512, 2048], replicated, may hold values from -0.1875 to 0.1875
- out_narrow: bfloat16 [512, 2048], replicated, may hold values from -0.1875 to 0.1875
- norm_gain: float32 [2048], replicated, may hold values from 0.1 to 1.9
- routing: int32 [16384, 2], P(('sp', 'tp')), may hold values from 0 to 63, as said below
- route_weight: float32 [16384, 2], P(('sp', 'tp')), may hold values from 0.3 to 1.5
- gate_weight: bfloat16 [64, 2048, 1024], P('sp', None, 'tp'), may hold values from -0.125 to 0.125
- up_weight: bfloat16 [64, 2048, 1024], P('sp', None, 'tp'), may hold values from -0.125 to 0.125
- down_weight: bfloat16 [64, 1024, 2048], P('sp', 'tp'), may hold values from -0.1875 to 0.1875
Outputs:
- result: bfloat16 [16384, 2048], P(('sp', 'tp'))
Inputs may be any that keep to these rules, and one draw needn't show every extreme that they name: `routing`: each row names 2 different experts of one group (experts g * 16 to g * 16 + 15). In each aligned block of 64 rows (the rows of one device) no expert is named by more than 4 rows; one group, the same for all blocks, has each of its experts named by exactly 4 rows of every block.
All inputs are finite; a program needn't handle non-finite values.
Results may differ from a plain program's by a relative error of at most 0.017.
Values may be sent and summed in bfloat16 or wider, within the bound.
No kernel may reach another device: no remote copies, remote signals or barrier semaphores. Data moves between devices by JAX's collectives and lax.ppermute only.
A program may use at most 128 MiB of HBM per device.

v0:
```python
import math

import jax
import jax.numpy as jnp
from jax import lax
from jax.sharding import PartitionSpec as P

HW = 128
HN = 64
GROUPS = 4


epsilon = 1e-06


def sent_together(arrays, axis, dim, along):
    both = jnp.concatenate(arrays, axis=along)
    whole, at, outs = (lax.all_gather(both, axis, axis=dim, tiled=True), 0, [])
    for a in arrays:
        outs.append(lax.slice_in_dim(whole, at, at + a.shape[along], axis=along))
        at += a.shape[along]
    return tuple(outs)


def globalize(pieces, shard_rows):
    shards = pieces.shape[0] // shard_rows
    grid = pieces.reshape(shards, shard_rows, pieces.shape[1])
    endings = grid[:, -1, :]
    offsets = jnp.cumsum(endings, axis=0) - endings
    return (grid + offsets[:, None, :]).reshape(pieces.shape)


def head_block(
    state, queries, query_decay, keys, values, key_decay, first_key, first_query, head_width
):
    highest_old, weight_sum, weighted = state
    query_rows = queries.shape[0]
    head_count = query_decay.shape[1]
    key_rows = keys.shape[0]
    grid_query = queries.reshape(query_rows, head_count, head_width)
    grid_key = keys.reshape(key_rows, head_count, head_width)
    grid_value = values.reshape(key_rows, head_count, head_width)
    scores = jnp.einsum("thd,phd->htp", grid_query, grid_key, preferred_element_type=jnp.float32)
    scores = scores * head_width ** (-0.5) + query_decay.T[:, :, None] - key_decay.T[:, None, :]
    query_place = first_query + jnp.arange(query_rows, dtype=jnp.int32)
    key_place = first_key + jnp.arange(key_rows, dtype=jnp.int32)
    scores = jnp.where(key_place[None, None, :] <= query_place[None, :, None], scores, -jnp.inf)
    highest = jnp.maximum(highest_old, jnp.max(scores, axis=2))
    weights = jnp.exp(scores - highest[:, :, None])
    shrink = jnp.exp(highest_old - highest)
    weight_sum = weight_sum * shrink + jnp.sum(weights, axis=2)
    product = jnp.einsum(
        "htp,phd->htd", weights.astype(jnp.bfloat16), grid_value, preferred_element_type=jnp.float32
    )
    weighted = weighted * shrink[:, :, None] + product
    return (highest, weight_sum, weighted)


def fresh_state(head_count, shard_rows, head_width):
    return (
        jnp.full((head_count, shard_rows), -1e30, jnp.float32),
        jnp.zeros((head_count, shard_rows), jnp.float32),
        jnp.zeros((head_count, shard_rows, head_width), jnp.float32),
    )


def finish(state, shard_rows):
    highest, weight_sum, weighted = state
    mixed_heads = weighted / weight_sum[:, :, None]
    joined = jnp.transpose(mixed_heads, (1, 0, 2))
    return joined.reshape(shard_rows, weighted.shape[0] * weighted.shape[2]).astype(jnp.bfloat16)


def body(
    residual,
    query_wide,
    key_wide,
    value_wide,
    query_narrow,
    key_narrow,
    value_narrow,
    gate_wide,
    gate_narrow,
    out_wide,
    out_narrow,
    norm_gain,
    routing,
    route_weight,
    gate_weight,
    up_weight,
    down_weight,
):
    shard_rows = query_wide.shape[0]
    half_rows = shard_rows // 2
    sp_place = lax.axis_index("sp")
    first_query = sp_place * shard_rows
    running_wide = jnp.cumsum(jax.nn.log_sigmoid(gate_wide), axis=0)
    running_narrow = jnp.cumsum(jax.nn.log_sigmoid(gate_narrow), axis=0)
    pieces_wide, pieces_narrow = sent_together((running_wide, running_narrow), "sp", 0, 1)
    every_wide = globalize(pieces_wide, shard_rows)
    every_narrow = globalize(pieces_narrow, shard_rows)
    late_first = first_query + half_rows
    halves = []
    for place, part_wide, part_narrow in (
        (first_query, query_wide[:half_rows], query_narrow[:half_rows]),
        (late_first, query_wide[half_rows:], query_narrow[half_rows:]),
    ):
        halves.append(
            (
                place,
                part_wide,
                part_narrow,
                lax.dynamic_slice_in_dim(every_wide, place, half_rows, 0),
                lax.dynamic_slice_in_dim(every_narrow, place, half_rows, 0),
            )
        )

    def half_state():
        return (
            fresh_state(gate_wide.shape[1], half_rows, HW),
            fresh_state(gate_narrow.shape[1], half_rows, HN),
        )

    state = (half_state(), half_state())
    keys_wide, values_wide, keys_narrow, values_narrow = sent_together(
        (key_wide, value_wide, key_narrow, value_narrow), "sp", 0, 1
    )
    span_rows = keys_wide.shape[0]
    block_size = math.gcd(span_rows, 2048)

    def visit(carried, position):
        inside = position * block_size

        def take_block(source):
            return lax.dynamic_slice_in_dim(source, inside, block_size, 0)

        def take_decay(source):
            return lax.dynamic_slice_in_dim(source, inside, block_size, 0)

        block_kw = take_block(keys_wide)
        block_vw = take_block(values_wide)
        block_kn = take_block(keys_narrow)
        block_vn = take_block(values_narrow)
        block_dw = take_decay(every_wide)
        block_dn = take_decay(every_narrow)

        def one_half(current, half):
            place, part_wide, part_narrow, query_decay_wide, query_decay_narrow = half

            def work(inner):
                first = head_block(
                    inner[0],
                    part_wide,
                    query_decay_wide,
                    block_kw,
                    block_vw,
                    block_dw,
                    inside,
                    place,
                    HW,
                )
                second = head_block(
                    inner[1],
                    part_narrow,
                    query_decay_narrow,
                    block_kn,
                    block_vn,
                    block_dn,
                    inside,
                    place,
                    HN,
                )
                return (first, second)

            def skip(inner):
                return inner

            return lax.cond(inside <= place + half_rows - 1, work, skip, current)

        updated = (one_half(carried[0], halves[0]), one_half(carried[1], halves[1]))
        return (updated, None)

    state, _ = lax.scan(visit, state, jnp.arange(span_rows // block_size, dtype=jnp.int32))
    att_wide = jnp.concatenate(
        [finish(state[0][0], half_rows), finish(state[1][0], half_rows)], axis=0
    )
    att_narrow = jnp.concatenate(
        [finish(state[0][1], half_rows), finish(state[1][1], half_rows)], axis=0
    )
    own_rows = residual.shape[0]
    heads_wide, heads_narrow = (
        lax.all_to_all(att_wide, "tp", split_axis=0, concat_axis=1, tiled=True),
        lax.all_to_all(att_narrow, "tp", split_axis=0, concat_axis=1, tiled=True),
    )
    mixed = jnp.dot(heads_wide, out_wide, preferred_element_type=jnp.float32)
    mixed = mixed + jnp.dot(heads_narrow, out_narrow, preferred_element_type=jnp.float32)
    middle = (residual.astype(jnp.float32) + mixed).astype(jnp.bfloat16)
    middle_wide = middle.astype(jnp.float32)
    spread = jnp.mean(middle_wide * middle_wide, axis=1, keepdims=True)
    normed = (middle_wide * lax.rsqrt(spread + epsilon) * norm_gain).astype(jnp.bfloat16)
    features = normed.shape[1]
    chosen_count = routing.shape[1]
    expert_count = gate_weight.shape[0] * lax.axis_size("sp")
    capacity = own_rows * GROUPS // expert_count
    flat_routes = routing.reshape(-1)
    matches = (flat_routes[:, None] == jnp.arange(expert_count, dtype=jnp.int32)[None, :]).astype(
        jnp.int32
    )
    ranking = jnp.sum((jnp.cumsum(matches, axis=0) - matches) * matches, axis=1)
    placing = flat_routes * capacity + ranking
    picker = (
        placing[None, :] == jnp.arange(expert_count * capacity, dtype=jnp.int32)[:, None]
    ).astype(jnp.bfloat16)
    picker = jnp.sum(picker.reshape(expert_count * capacity, own_rows, chosen_count), axis=2)
    outgoing = jnp.dot(picker, normed, preferred_element_type=jnp.float32).astype(jnp.bfloat16)
    outgoing = outgoing.reshape(expert_count, capacity, features)
    arrived = lax.all_to_all(outgoing, "sp", split_axis=0, concat_axis=0, tiled=True)
    pooled = lax.all_gather(arrived.reshape(-1, features), "tp", axis=0, tiled=True)
    gate_value = jnp.dot(pooled, gate_weight[0], preferred_element_type=jnp.float32)
    up_value = jnp.dot(pooled, up_weight[0], preferred_element_type=jnp.float32)
    hidden = (jax.nn.silu(gate_value) * up_value).astype(jnp.bfloat16)
    answers = lax.psum_scatter(
        jnp.dot(hidden, down_weight[0], preferred_element_type=jnp.float32).astype(jnp.bfloat16),
        "tp",
        scatter_dimension=0,
        tiled=True,
    )
    returned = lax.all_to_all(
        answers.reshape(expert_count, capacity, features),
        "sp",
        split_axis=0,
        concat_axis=0,
        tiled=True,
    )
    picked = jnp.take(returned.reshape(expert_count * capacity, features), placing, axis=0)
    picked = picked.reshape(own_rows, chosen_count, features).astype(jnp.float32)
    combined = jnp.sum(route_weight[:, :, None] * picked, axis=1)
    return (middle_wide + combined).astype(jnp.bfloat16)


def solution(mesh):
    placed = (
        P(("sp", "tp"), None),
        P("sp", "tp"),
        P("sp", "tp"),
        P("sp", "tp"),
        P("sp", "tp"),
        P("sp", "tp"),
        P("sp", "tp"),
        P("sp", "tp"),
        P("sp", "tp"),
        P(),
        P(),
        P(),
        P(("sp", "tp"), None),
        P(("sp", "tp"), None),
        P("sp", None, "tp"),
        P("sp", None, "tp"),
        P("sp", "tp", None),
    )
    return jax.shard_map(
        body, mesh=mesh, in_specs=placed, out_specs=P(("sp", "tp"), None), check_vma=False
    )
```

profile of v0, /device:TPU:1, one launch (start us, length us, event | category | flops | bytes accessed | tf_op | source)
XLA Modules:
  0.0 530.6 jit_solution(731115562800236567)
XLA Ops:
  18.2 48.7 %all_gather.10 = f32[16384,3]{0,1:T(4,128)S(1)} all-gather(f32[256,3]{0,1:T(4,128)S(1)} %pad_maximum_fusion.3), channel_id=1, replica_groups=mesh['sp'=64,'tp'=4] {'sp'}, dimensions={0}, use_global_device_ids=true | all-gather | bytes 199680 | tf_op jit(solution)/shard_map/all_gather | solution.py:18
  67.1 4.9 copy.106
  73.7 9.2 %reshape.388 = f32[64,256,1]{2,1,0:T(8,128)} reshape(f32[16384]{0:T(1024)S(1)} %slice_reduce_fusion) | data formatting | bytes 131072 | tf_op jit(solution)/shard_map/reshape | solution.py:27
  89.4 32.0 %all-gather.3.cloned.1.call-done = bf16[16384,512]{0,1:T(8,128)(2,1)} async-done(((bf16[256,512]{0,1:T(8,128)(2,1)}), bf16[16384,512]{0,1:T(8,128)(2,1)}) %all-gather.3.cloned.1.call-update) | async-done | bytes 16777232 | tf_op jit(solution)/shard_map/all_gather | solution.py:18
  121.4 12.1 %fusion.72 = (bf16[16384,128]{0,1:T(8,128)(2,1)}, bf16[16384,128]{0,1:T(8,128)(2,1)}, bf16[16384,128]{0,1:T(8,128)(2,1)}, bf16[16384,128]{0,1:T(8,128)(2,1)}) fusion(bf16[16384,512]{0,1:T(8,128)(2,1)} %all-gather.3.cloned.1.call-done), kind=kLoop, calls=%fused_computation.146 | loop fusion | bytes 33554432 | tf_op jit(solution)/shard_map/slice | solution.py:20
  138.6 89.0 %while.35 = (s32[]{:T(128)}, f32[1,128]{1,0:T(1,128)}, f32[1,128]{1,0:T(1,128)}, f32[1,128,128]{2,1,0:T(8,128)S(1)}, f32[2,128]{1,0:T(2,128)}, /*index=5*/f32[2,...) while((s32[]{:T(128)}, f32[1,128]{1,0:T(1,128)}, ...), condition=%wide.region_19.20_spmd, body=%wide.region_6.19_spmd.sunk | while | flops 552212480 | bytes 35769752 | solution.py:183
  143.8 2.1 constant_dynamic-slice_fusion.14
  148.2 5.7 %conditional.4 = ((f32[1,128]{1,0:T(1,128)}, f32[1,128]{1,0:T(1,128)}, f32[1,128,128]{2,1,0:T(8,128)S(1)}, f32[2,128]{1,0:T(2,128)}, f32[2,128]{1,0:T(2,128)}, /*index=5*/f32[2,128,64]{1,2,0:T(8,128)S(1)})) conditional(s32[]{:T(128)} %convert_element_type.151, (f32[1,128]{1,0:T(1,128)}, f32[1,128]{1,0:T(1,128)}, f32[1,128,128]{2,1,0:T(8,128)S(1)}, ...), branch_computations={%region_7.7_spmd, %region_8.12_spmd} | conditional | flops 276106240 | bytes 14714172 | solution.py:178
  153.9 5.6 %conditional.5 = ((f32[1,128]{1,0:T(1,128)}, f32[1,128]{1,0:T(1,128)}, f32[1,128,128]{2,1,0:T(8,128)S(1)}, f32[2,128]{1,0:T(2,128)}, f32[2,128]{1,0:T(2,128)}, /*index=5*/f32[2,128,64]{1,2,0:T(8,128)S(1)})) conditional(s32[]{:T(128)} %convert_element_type.152, (f32[1,128]{1,0:T(1,128)}, f32[1,128]{1,0:T(1,128)}, f32[1,128,128]{2,1,0:T(8,128)S(1)}, ...), branch_computations={%region_13.13_spmd, %region_14.18_spmd} | conditional | flops 276106240 | bytes 14714172 | solution.py:178
  162.7 2.1 constant_dynamic-slice_fusion.16
  164.7 2.1 constant_dynamic-slice_fusion.14
  172.4 2.1 constant_dynamic-slice_fusion.16
  174.5 2.1 constant_dynamic-slice_fusion.14
  184.2 2.1 constant_dynamic-slice_fusion.14
  193.9 2.1 constant_dynamic-slice_fusion.14
  203.7 2.1 constant_dynamic-slice_fusion.14
  213.4 2.1 constant_dynamic-slice_fusion.14
  223.1 2.1 constant_dynamic-slice_fusion.14
  229.1 4.1 all-to-all-start
  234.6 3.0 all-to-all-done
  237.6 3.3 all-to-all-start.1
  241.2 2.1 fusion.53
  243.2 2.1 all-to-all-done.1
  248.5 115.7 %all_to_all.48 = bf16[64,4,2048]{2,1,0:T(4,128)(2,1)S(1)} all-to-all(bf16[64,4,2048]{2,1,0:T(4,128)(2,1)} %reshape.376), channel_id=1, replica_groups=mesh['sp'=64,'tp'=4] {'sp'}, dimensions={0} | all-to-all | bytes 2097152 | tf_op jit(solution)/shard_map/all_to_all | solution.py:217
  365.3 45.8 %all-gather.5.cloned.1.call-done = bf16[1024,2048]{1,0:T(8,128)(2,1)} async-done(((bf16[256,2048]{1,0:T(8,128)(2,1)}), bf16[1024,2048]{1,0:T(8,128)(2,1)}) %all-gather.5.cloned.1.call-update) | async-done | bytes 4194320 | tf_op jit(solution)/shard_map/all_gather | solution.py:218
  411.1 4.8 fusion.39
  415.9 9.1 %convolution_convert_fusion = bf16[1024,2048]{1,0:T(8,128)(2,1)} fusion(bf16[1024,2048]{1,0:T(8,128)(2,1)} %all-gather.5.cloned.1.call-done, bf16[1,256,2048]{2,1,0:T(8,128)(2,1)S(1)} %copy-done.31, bf16[1,2048,256]{2,1,0:T(8,128)(2,1)} %param.38, f32[1024,256]{1,0:T(8,128)} %fusion.39), kind=kOutput, calls=%fused_computation.63 | convolution fusion | flops 2151153664 | bytes 11534336 | tf_op jit(solution)/shard_map/dot_general | solution.py:223
  425.0 50.0 %reduce-scatter.2.cloned.1.call-done = bf16[256,2048]{1,0:T(8,128)(2,1)} async-done(((bf16[1024,2048]{1,0:T(8,128)(2,1)}), bf16[256,2048]{1,0:T(8,128)(2,1)}) %reduce-scatter.2.cloned.1.call-update) | async-done | bytes 1048592 | tf_op jit(solution)/shard_map/reduce_scatter | solution.py:222
  475.0 2.2 reshape.378
  477.2 10.9 %all-to-all-start.3 = ((bf16[64,4,2048]{2,1,0:T(4,128)(2,1)}), bf16[64,4,2048]{2,1,0:T(4,128)(2,1)}, u32[]{:S(2)}, u32[]{:S(2)}) async-start(bf16[64,4,2048]{2,1,0:T(4,128)(2,1)} %reshape.378), calls=%async_computation.4 | async-start | bytes 2097152 | tf_op jit(solution)/shard_map/all_to_all | solution.py:228
  488.7 27.6 %all-to-all-done.3 = bf16[64,4,2048]{2,1,0:T(4,128)(2,1)} async-done(((bf16[64,4,2048]{2,1,0:T(4,128)(2,1)}), bf16[64,4,2048]{2,1,0:T(4,128)(2,1)}, u32[]{:S(2)}, u32[]{:S(2)}) %all-to-all-start.3) | async-done | bytes 1048608 | tf_op jit(solution)/shard_map/all_to_all | solution.py:228
  520.7 2.5 multiply_reduce_fusion
  (240 shorter events, 100.0 us)
Async XLA Ops:
  6.5 238.8 %copy-start = (bf16[512,2048]{1,0:T(8,128)(2,1)S(1)}, bf16[512,2048]{1,0:T(8,128)(2,1)}, u32[]{:S(2)}) copy-start(bf16[512,2048]{1,0:T(8,128)(2,1)} %param.33) | copy-start | bytes 6291460
  6.5 114.8 %all-gather.3.cloned.1.call-start = ((), (), s32[]{:S(2)}) async-start(), calls=%async_computation.5 | async-start | bytes 17039360 | tf_op jit(solution)/shard_map/all_gather | solution.py:18
  14.3 3.9 copy-start.25
  73.7 13.8 %copy-start.22 = (s32[64,2]{0,1:T(2,128)S(1)}, s32[64,2]{0,1:T(2,128)}, u32[]{:S(2)}) copy-start(s32[64,2]{0,1:T(2,128)} %param.35) | copy-start | bytes 1540
  73.7 15.0 %copy-start.9 = (bf16[256,128]{1,0:T(8,128)(2,1)S(1)}, bf16[256,128]{1,0:T(8,128)(2,1)}, u32[]{:S(2)}) copy-start(bf16[256,128]{1,0:T(8,128)(2,1)} %param.24) | copy-start | bytes 196612
  148.3 1.9 copy-start.11
  148.5 2.3 copy-start.20
  148.5 2.9 copy-start.1
  148.5 2.9 copy-start.17
  148.5 2.9 copy-start.30
  150.8 1.5 copy-start.8
  150.8 1.4 copy-start.21
  153.9 1.8 copy-start.10
  154.2 2.3 copy-start.18
  154.2 2.8 copy-start.2
  154.2 2.8 copy-start.16
  154.2 2.8 copy-start.29
  156.5 1.4 copy-start.7
  227.6 17.8 %copy-start.5 = (bf16[64,2048]{1,0:T(8,128)(2,1)S(1)}, bf16[64,2048]{1,0:T(8,128)(2,1)}, u32[]{:S(2)}) copy-start(bf16[64,2048]{1,0:T(8,128)(2,1)} %param.23) | copy-start | bytes 786436
  229.1 8.6 %all-to-all-start = ((bf16[4,64,128]{2,1,0:T(8,128)(2,1)}), bf16[4,64,128]{2,1,0:T(8,128)(2,1)S(1)}, u32[]{:S(2)}, u32[]{:S(2)}) async-start(bf16[4,64,128]{2,1,0:T(8,128)(2,1)} %bitcast.37), calls=%async_computation | async-start | bytes 131072 | tf_op jit(solution)/shard_map/all_to_all | solution.py:192
  237.6 7.7 %all-to-all-start.1 = ((bf16[4,64,128]{2,1,0:T(8,128)(2,1)}), bf16[4,64,128]{2,1,0:T(8,128)(2,1)S(1)}, u32[]{:S(2)}, u32[]{:S(2)}) async-start(bf16[4,64,128]{2,1,0:T(8,128)(2,1)} %bitcast.43), calls=%async_computation.1 | async-start | bytes 131072 | tf_op jit(solution)/shard_map/all_to_all | solution.py:193
  240.9 170.2 %all-gather.5.cloned.1.call-start = ((), (), s32[]{:S(2)}) async-start(), calls=%async_computation.6 | async-start | bytes 5242880 | tf_op jit(solution)/shard_map/all_gather | solution.py:218
  243.2 3.6 copy-start.6
  243.2 3.6 copy-start.24
  365.3 50.6 %copy-start.31 = (bf16[1,256,2048]{2,1,0:T(8,128)(2,1)S(1)}, bf16[1,256,2048]{2,1,0:T(8,128)(2,1)}, u32[]{:S(2)}) copy-start(bf16[1,256,2048]{2,1,0:T(8,128)(2,1)} %param.39) | copy-start | bytes 3145732
  365.3 109.7 %reduce-scatter.2.cloned.1.call-start = ((), (), s32[]{:S(2)}) async-start(), calls=%async_computation.7 | async-start | bytes 5242880 | tf_op jit(solution)/shard_map/reduce_scatter | solution.py:222
  425.0 63.2 %copy-start.23 = (s32[64,2]{0,1:T(2,128)S(1)}, s32[64,2]{0,1:T(2,128)}, u32[]{:S(2)}) copy-start(s32[64,2]{0,1:T(2,128)} %param.35) | copy-start | bytes 1540
  425.0 63.4 %copy-start.28 = (f32[64,2]{0,1:T(2,128)S(1)}, f32[64,2]{0,1:T(2,128)}, u32[]{:S(2)}) copy-start(f32[64,2]{0,1:T(2,128)} %param.36) | copy-start | bytes 1540
  425.0 63.5 %copy-start.27 = (pred[64,2]{0,1:T(4,128)(4,1)S(1)}, pred[64,2]{0,1:T(4,128)(4,1)}, u32[]{:S(2)}) copy-start(pred[64,2]{0,1:T(4,128)(4,1)} %get-tuple-element.875) | copy-start | bytes 388
  425.0 63.6 %copy-start.26 = (s32[128]{0:T(128)S(1)}, s32[128]{0:T(128)}, u32[]{:S(2)}) copy-start(s32[128]{0:T(128)} %copy-done.25) | copy-start | bytes 1540
  477.2 39.0 %all-to-all-start.3 = ((bf16[64,4,2048]{2,1,0:T(4,128)(2,1)}), bf16[64,4,2048]{2,1,0:T(4,128)(2,1)}, u32[]{:S(2)}, u32[]{:S(2)}) async-start(bf16[64,4,2048]{2,1,0:T(4,128)(2,1)} %reshape.378), calls=%async_computation.4 | async-start | bytes 2097152 | tf_op jit(solution)/shard_map/all_to_all | solution.py:228
  519.3 4.0 copy-start.4
  (6 other events, 7.1 us)
Sparse Core Ops, SparseCore 0:
  11.3 110.0 all-gather.2
  365.4 45.6 all-gather.4
  425.1 49.8 reduce-scatter.1
where the time goes:
time: 533 us; the launch traced here: 531 us
  blocking collectives  164 us (31%)
  waiting for transfers between devices  161 us (30%)
  local copies, waits for them, and re-layouts  127 us (24%)
  matrix products  23.7 us (4%)
  starting transfers between devices  18.5 us (3%)
  other arithmetic  16.4 us (3%)
  between operations  13.5 us (3%)
  loops' own time  6.28 us (1%)
    all_to_all x1, blocking collectives, body(): lax.all_to_all(outgoing, 'sp', split_axis=0, concat_axis=0, tiled=True)  116 us
    dynamic_slice x32, local copies, waits for them, and re-layouts, take_block(): return lax.dynamic_slice_in_dim(source, inside, block_size, 0)  51.8 us
    reduce_scatter x1, waiting for transfers between devices, body(): lax.psum_scatter(jnp.dot(hidden, down_weight[0], preferred_element_type=j...  50 us
    all_gather x1, blocking collectives, sent_together(): whole, at, outs = (lax.all_gather(both, axis, axis=dim, tiled=True), 0, [])  48.7 us
    all_gather x1, waiting for transfers between devices, body(): lax.all_gather(arrived.reshape(-1, features), 'tp', axis=0, tiled=True)  45.8 us
    all_gather x1, waiting for transfers between devices, sent_together(): whole, at, outs = (lax.all_gather(both, axis, axis=dim, tiled=True), 0, [])  32 us
    all_to_all x1, waiting for transfers between devices, body(): lax.all_to_all(answers.reshape(expert_count, capacity, features), 'sp', s...  27.6 us
    slice x4, local copies, waits for them, and re-layouts, sent_together(): outs.append(lax.slice_in_dim(whole, at, at + a.shape[along], axis=along))  17.3 us
  transfers between devices with their start and end apart: 6, of which 6 were waited for; matrix products, arithmetic and copies ran while one was open for 6% of the time, Pallas kernels for 0%

commit v1 on v0

v1 whole, which is shorter than its diff:
```python
import functools

import jax
import jax.numpy as jnp
from jax import lax
from jax.experimental import pallas as pl
from jax.experimental.pallas import tpu as pltpu
from jax.sharding import Mesh
from jax.sharding import PartitionSpec as P

HW = 128
HN = 64
GROUPS = 4
EPS = 1e-06
LOG2E = 1.4426950408889634
LOW = -1e30
TQ = 256


def dot_f32(a, b, dims=(((1,), (0,)), ((), ()))):
    return lax.dot_general(a, b, dims, preferred_element_type=jnp.float32)


def attention_kernel(
    place_ref, q_ref, dk_ref, kv_ref, *rest, flip, row0, rows, dev_rows, tiles, first, last
):
    if first:
        ins, rest = (), rest
    else:
        ins, rest = rest[:3], rest[3:]
    if last:
        out_ref, m_ref, l_ref, acc_ref, qh_ref = rest
    else:
        m_ref, l_ref, acc_ref, qh_ref = rest
    t = pl.program_id(0)
    place = place_ref[0]
    chip, core = place // 2, place % 2
    sub = core if flip == 0 else 1 - core
    tile_keys = kv_ref.shape[0]
    chips_tile = tile_keys // rows
    last_tile = chip // chips_tile
    queries = q_ref.shape[0]
    scale = jnp.where(core == 0, jnp.float32(HW**-0.5 * LOG2E), jnp.float32(HN**-0.5 * LOG2E))

    @pl.when(t == 0)
    def _():
        if first:
            m_ref[...] = jnp.full_like(m_ref, LOW)
            l_ref[...] = jnp.zeros_like(l_ref)
            acc_ref[...] = jnp.zeros_like(acc_ref)
        else:
            m_ref[...] = ins[0][...]
            l_ref[...] = ins[1][...]
            acc_ref[...] = ins[2][...]
        lane = lax.broadcasted_iota(jnp.int32, (queries, HW), 1)
        q = q_ref[...]
        zero = jnp.zeros_like(q)
        qh_ref[0] = jnp.where((core == 0) | (lane < HN), q, zero)
        qh_ref[1] = jnp.where(lane >= HN, q, zero)

    def one(h, masked):
        k = kv_ref[:, :HW]
        v = kv_ref[:, HW:]
        lines = dev_rows // 128
        dk = jnp.concatenate(
            [
                dk_ref[2 * c + sub, pl.ds(lines * (h + core) + (row0 + r) // 128, 1), :]
                for c in range(chips_tile)
                for r in range(0, rows, 128)
            ],
            axis=1,
        )
        for r0 in range(0, queries, TQ):
            span = pl.ds(r0, TQ)
            s = dot_f32(qh_ref[h, span, :], k, (((1,), (1,)), ((), ()))) * scale - dk
            if masked:
                col = lax.broadcasted_iota(jnp.int32, (TQ, tile_keys), 1)
                row = lax.broadcasted_iota(jnp.int32, (TQ, tile_keys), 0)
                key_chip = t * chips_tile + col // rows
                key_place = key_chip * (2 * dev_rows) + sub * dev_rows + row0 + col % rows
                s = jnp.where(key_place <= chip * (2 * dev_rows) + r0 + row, s, LOW)
            m_old = m_ref[h, span, :]
            m_new = jnp.maximum(m_old, jnp.max(s, axis=1, keepdims=True))
            alpha = jnp.exp2(m_old - m_new)
            p = jnp.exp2(s - m_new[:, :1])
            m_ref[h, span, :] = m_new
            l_ref[h, span, :] = l_ref[h, span, :] * alpha + jnp.sum(p, axis=1, keepdims=True)
            acc_ref[h, span, :] = acc_ref[h, span, :] * alpha + dot_f32(p.astype(jnp.bfloat16), v)

    for masked in (False, True):
        at = (t == last_tile) if masked else (t < last_tile)

        @pl.when(at)
        def _():
            one(0, masked)

        @pl.when(at & (core == 1))
        def _():
            one(1, masked)

    if last:

        @pl.when(t == tiles - 1)
        def _():
            one_head = acc_ref[0] / l_ref[0]
            lane = lax.broadcasted_iota(jnp.int32, (queries, HW), 1)
            other = acc_ref[1] / jnp.where(core == 0, 1.0, l_ref[1])
            out_ref[...] = jnp.where((core == 0) | (lane < HN), one_head, other).astype(jnp.bfloat16)


def attend_chunk(place, q, dk, kv, state, flip, row0, rows, dev_rows, last):
    queries = q.shape[0]
    keys = kv.shape[0]
    tile_keys = min(1024, keys)
    chips_tile = tile_keys // rows
    tiles = keys // tile_keys
    first = state is None

    def clamp(t, place):
        return jnp.minimum(t, place[0] // 2 // chips_tile)

    whole = pl.BlockSpec((2, queries, HW), lambda t, place: (0, 0, 0))
    in_specs = [
        pl.BlockSpec((queries, HW), lambda t, place: (0, 0)),
        pl.BlockSpec((2 * chips_tile, *dk.shape[1:]), lambda t, place: (clamp(t, place), 0, 0)),
        pl.BlockSpec((tile_keys, 2 * HW), lambda t, place: (clamp(t, place), 0)),
    ]
    args = [q, dk, kv]
    if not first:
        in_specs += [whole] * 3
        args += list(state)
    held = jax.ShapeDtypeStruct((2, queries, HW), jnp.float32)
    scratch = [pltpu.VMEM((2, queries, HW), jnp.bfloat16)]
    if last:
        out_shape = jax.ShapeDtypeStruct((queries, HW), jnp.bfloat16)
        out_specs = pl.BlockSpec((queries, HW), lambda t, place: (0, 0))
        scratch = [pltpu.VMEM((2, queries, HW), jnp.float32)] * 3 + scratch
    else:
        out_shape = [held] * 3
        out_specs = [whole] * 3
    return pl.pallas_call(
        functools.partial(
            attention_kernel,
            flip=flip,
            row0=row0,
            rows=rows,
            dev_rows=dev_rows,
            tiles=tiles,
            first=first,
            last=last,
        ),
        out_shape=out_shape,
        grid_spec=pltpu.PrefetchScalarGridSpec(
            num_scalar_prefetch=1,
            grid=(tiles,),
            in_specs=in_specs,
            out_specs=out_specs,
            scratch_shapes=scratch,
        ),
        compiler_params=pltpu.CompilerParams(
            dimension_semantics=("arbitrary",), vmem_limit_bytes=60 * 1024 * 1024
        ),
        cost_estimate=pl.CostEstimate(
            flops=8 * queries * keys * HW, transcendentals=2 * queries * keys, bytes_accessed=4 * keys * HW
        ),
        name="attend",
    )(place, *args)


def running_kernel(wide_ref, narrow_ref, out_ref):
    gates = jnp.concatenate([wide_ref[...], narrow_ref[...]], axis=0)
    kept = jnp.minimum(gates, 0.0) - jnp.log1p(jnp.exp(-jnp.abs(gates)))
    heads, rows = kept.shape
    row = lax.broadcasted_iota(jnp.int32, (rows, rows), 0)
    col = lax.broadcasted_iota(jnp.int32, (rows, rows), 1)
    upto = (row <= col).astype(jnp.float32)
    kept = jnp.concatenate([kept, jnp.zeros((8 - heads, rows), jnp.float32)], axis=0)
    sums = lax.dot_general(
        kept,
        upto,
        (((1,), (0,)), ((), ())),
        precision=lax.Precision.HIGHEST,
        preferred_element_type=jnp.float32,
    )
    out_ref[...] = jnp.zeros_like(out_ref)
    lines = rows // 128
    for h in range(heads):
        for j in range(lines):
            at = lines * h + j
            out_ref[at : at + 1, :] = sums[h : h + 1, j * 128 : (j + 1) * 128]


def running_sums(gate_wide, gate_narrow):
    return pl.pallas_call(
        running_kernel, out_shape=jax.ShapeDtypeStruct((8, 128), jnp.float32), name="running"
    )(gate_wide.T, gate_narrow.T)


def offset_kernel(place_ref, every_ref, out_ref):
    home = place_ref[0] // 2 * 2
    devices = every_ref.shape[0]
    odd = lax.broadcasted_iota(jnp.int32, (8, 128), 0) % 2 == 1
    offset = jnp.zeros((8, 128), jnp.float32)
    base = offset
    for d in range(devices):
        here = every_ref[d]
        out_ref[d] = here + offset
        base = jnp.where(home == d, offset, base)
        end = jnp.broadcast_to(here[:, 127:128], (8, 128))
        offset = offset + jnp.where(odd, end, jnp.concatenate([end[1:], end[:1]], axis=0))
    for d in range(devices):
        out_ref[d] = (out_ref[d] - base) * LOG2E


def offset_sums(place, every):
    return pl.pallas_call(
        offset_kernel,
        out_shape=jax.ShapeDtypeStruct(every.shape, jnp.float32),
        in_specs=[pl.BlockSpec(memory_space=pltpu.SMEM), pl.BlockSpec(memory_space=pltpu.VMEM)],
        name="offset",
    )(place, every)


def placed_slots(routing, experts, capacity):
    rows = routing.shape[0]
    expert = lax.broadcasted_iota(jnp.int32, (rows, experts), 1)
    hits = [(routing[:, k : k + 1] == expert).astype(jnp.float32) for k in range(2)]
    row = lax.broadcasted_iota(jnp.int32, (rows, rows), 0)
    col = lax.broadcasted_iota(jnp.int32, (rows, rows), 1)
    before = (col < row).astype(jnp.bfloat16)
    earlier = dot_f32(before, (hits[0] + hits[1]).astype(jnp.bfloat16))
    slot = lax.broadcasted_iota(jnp.int32, (rows, 2 * experts * capacity), 1)
    picks = []
    for k in range(2):
        rank = jnp.sum(earlier * hits[k], axis=1, keepdims=True).astype(jnp.int32)
        place = routing[:, k : k + 1] * (2 * capacity) + rank
        picks.append([(place + half * capacity == slot).astype(jnp.bfloat16) for half in range(2)])
    return picks


def project_kernel(
    att_ref, wide_ref, narrow_ref, residual_ref, gain_ref, routing_ref, middle_ref, out_ref, *, experts, capacity
):
    half = att_ref.shape[0] // 2
    wide = jnp.concatenate([att_ref[j] for j in range(half)], axis=1)
    narrow = jnp.concatenate([att_ref[half + j] for j in range(half)], axis=1)
    mixed = dot_f32(wide, wide_ref[...]) + dot_f32(narrow, narrow_ref[...])
    middle = (residual_ref[...].astype(jnp.float32) + mixed).astype(jnp.bfloat16)
    middle_ref[...] = middle
    wider = middle.astype(jnp.float32)
    spread = jnp.mean(wider * wider, axis=1, keepdims=True)
    normed = (wider * lax.rsqrt(spread + EPS) * gain_ref[...]).astype(jnp.bfloat16)
    picks = placed_slots(routing_ref[...], experts, capacity)
    half = normed.shape[1] // 2
    over_rows = (((0,), (0,)), ((), ()))
    low = dot_f32(picks[0][0] + picks[1][0], normed[:, :half], over_rows)
    high = dot_f32(picks[0][1] + picks[1][1], normed[:, half:], over_rows)
    out_ref[...] = (low + high).astype(jnp.bfloat16)


def project(att, wide, narrow, residual, gain, routing, experts, capacity):
    rows, width = residual.shape
    return pl.pallas_call(
        functools.partial(project_kernel, experts=experts, capacity=capacity),
        out_shape=[
            jax.ShapeDtypeStruct((rows, width), jnp.bfloat16),
            jax.ShapeDtypeStruct((2 * experts * capacity, width // 2), jnp.bfloat16),
        ],
        compiler_params=pltpu.CompilerParams(vmem_limit_bytes=40 * 1024 * 1024),
        cost_estimate=pl.CostEstimate(
            flops=2 * rows * 1024 * width, transcendentals=0, bytes_accessed=2 * 1024 * width
        ),
        name="project",
    )(att, wide, narrow, residual, gain, routing)


def expert_kernel(x_ref, *rest, capacity):
    weights, (out_ref, g_ref, u_ref, d_ref, sems) = rest[:13], rest[13:]
    copies = []
    for j in range(4):
        mine = [
            pltpu.make_async_copy(weights[3 * j], g_ref.at[j], sems.at[j, 0]),
            pltpu.make_async_copy(weights[3 * j + 1], u_ref.at[j], sems.at[j, 1]),
        ]
        if j < 3:
            mine.append(pltpu.make_async_copy(weights[3 * j + 2], d_ref.at[j], sems.at[j, 2]))
        else:
            part = weights[11].shape[0]
            mine.append(pltpu.make_async_copy(weights[11], d_ref.at[j, pl.ds(0, part)], sems.at[j, 2]))
            mine.append(pltpu.make_async_copy(weights[12], d_ref.at[j, pl.ds(part, part)], sems.at[j, 3]))
        copies.append(mine)
    for mine in copies:
        for copy in mine:
            copy.start()
    x = x_ref[...]
    slots = x.shape[0]
    slot = lax.broadcasted_iota(jnp.int32, (slots // 2, slots), 0)
    from_slot = lax.broadcasted_iota(jnp.int32, (slots // 2, slots), 1)
    low_place = slot // capacity * (2 * capacity) + slot % capacity
    low = (from_slot == low_place).astype(jnp.bfloat16)
    high = (from_slot == low_place + capacity).astype(jnp.bfloat16)
    x = jnp.concatenate([dot_f32(low, x), dot_f32(high, x)], axis=1).astype(jnp.bfloat16)
    total = None
    for j in range(4):
        for copy in copies[j]:
            copy.wait()
        gate = dot_f32(x, g_ref[j])
        up = dot_f32(x, u_ref[j])
        hidden = (gate * jax.nn.sigmoid(gate) * up).astype(jnp.bfloat16)
        part = dot_f32(hidden, d_ref[j])
        total = part if total is None else total + part
    total = total.astype(jnp.bfloat16)
    half = total.shape[1] // 2
    over_rows = (((0,), (0,)), ((), ()))
    spread = dot_f32(low, total[:, :half], over_rows) + dot_f32(high, total[:, half:], over_rows)
    out_ref[...] = spread.astype(jnp.bfloat16)


def expert(x, weights, capacity):
    rows, width = x.shape[0] // 2, 2 * x.shape[1]
    units = weights[0].shape[1]
    anywhere = pl.BlockSpec(memory_space=pl.ANY)
    vmem = pl.BlockSpec(memory_space=pltpu.VMEM)
    return pl.pallas_call(
        functools.partial(expert_kernel, capacity=capacity),
        out_shape=jax.ShapeDtypeStruct(x.shape, jnp.bfloat16),
        in_specs=[vmem] + [anywhere] * 13,
        out_specs=vmem,
        scratch_shapes=[
            pltpu.VMEM((4, width, units), jnp.bfloat16),
            pltpu.VMEM((4, width, units), jnp.bfloat16),
            pltpu.VMEM((4, units, width), jnp.bfloat16),
            pltpu.SemaphoreType.DMA((4, 4)),
        ],
        compiler_params=pltpu.CompilerParams(vmem_limit_bytes=48 * 1024 * 1024),
        cost_estimate=pl.CostEstimate(
            flops=24 * rows * width * units, transcendentals=0, bytes_accessed=24 * width * units
        ),
        name="expert",
    )(x, *weights)


def combine_kernel(back_ref, middle_ref, routing_ref, weight_ref, out_ref, *, experts, capacity):
    picks = placed_slots(routing_ref[...], experts, capacity)
    back = back_ref[...]
    total = middle_ref[...].astype(jnp.float32)
    for k in range(2):
        answer = jnp.concatenate([dot_f32(picks[k][0], back), dot_f32(picks[k][1], back)], axis=1)
        total = total + weight_ref[:, k : k + 1] * answer
    out_ref[...] = total.astype(jnp.bfloat16)


def combine(back, middle, routing, weight, experts, capacity):
    return pl.pallas_call(
        functools.partial(combine_kernel, experts=experts, capacity=capacity),
        out_shape=jax.ShapeDtypeStruct(middle.shape, jnp.bfloat16),
        compiler_params=pltpu.CompilerParams(vmem_limit_bytes=24 * 1024 * 1024),
        name="combine",
    )(back, middle, routing, weight)


def body(
    residual,
    query_wide,
    key_wide,
    value_wide,
    query_narrow,
    key_narrow,
    value_narrow,
    gate_wide,
    gate_narrow,
    out_wide,
    out_narrow,
    norm_gain,
    routing,
    route_weight,
    gate_weight,
    up_weight,
    down_weight,
):
    dev_rows = query_wide.shape[0]
    own_rows, width = residual.shape
    core = lax.axis_index("core")
    is_wide = core == 0
    n_chip = lax.axis_size("chip")
    n_sp = 2 * n_chip
    n_tp = lax.axis_size("tp")
    place = jnp.full((1,), lax.axis_index(("chip", "core")), jnp.int32)

    def pick(a, b):
        return jnp.where(is_wide, a, b)

    keep = jnp.concatenate([pick(key_wide, key_narrow), pick(value_wide, value_narrow)], axis=1)
    give = jnp.concatenate([pick(key_narrow, key_wide), pick(value_narrow, value_wide)], axis=1)
    swap = [(0, 1), (1, 0)]
    got = lax.ppermute(give, "core", swap)
    q_keep = pick(query_wide, query_narrow)
    q_got = lax.ppermute(pick(query_narrow, query_wide), "core", swap)
    queries = jnp.concatenate([pick(q_keep, q_got), pick(q_got, q_keep)], axis=0)

    g, u, d = gate_weight[0], up_weight[0], down_weight[0]
    ahead = [(i, (i + 1) % n_tp) for i in range(n_tp)]
    behind = [(i, (i - 1) % n_tp) for i in range(n_tp)]
    from_left = [lax.ppermute(w, "tp", ahead) for w in (g, u, d)]
    from_right = [lax.ppermute(w, "tp", behind) for w in (g, u, d)]
    part = d.shape[0] // 2
    far = [
        lax.ppermute(from_left[0], "tp", ahead),
        lax.ppermute(from_right[1], "tp", behind),
        lax.ppermute(from_left[2][:part], "tp", ahead),
        lax.ppermute(from_right[2][part:], "tp", behind),
    ]

    chunk_a = lax.all_gather(keep, "chip", axis=0, tiled=True)
    chunk_b = lax.all_gather(got, "chip", axis=0, tiled=True)

    every = lax.all_gather(running_sums(gate_wide, gate_narrow), ("chip", "core"), axis=0)
    decay = offset_sums(place, every)

    state = attend_chunk(place, queries, decay, chunk_a, None, 0, 0, dev_rows, dev_rows, False)
    att = attend_chunk(place, queries, decay, chunk_b, state, 1, 0, dev_rows, dev_rows, True)

    att = lax.all_to_all(
        att.reshape(2 * n_tp, own_rows, HW), ("core", "tp"), split_axis=0, concat_axis=0, tiled=True
    )
    experts = n_sp
    capacity = own_rows * GROUPS // experts
    middle, outgoing = project(
        att, out_wide, out_narrow, residual, norm_gain.reshape(1, width), routing, experts, capacity
    )

    def exchange(slots):
        shape = slots.shape
        slots = slots.reshape(experts, 2 * capacity, width // 2)
        slots = lax.all_to_all(slots, ("chip", "core"), split_axis=0, concat_axis=0, tiled=True)
        return slots.reshape(shape)

    arrived = exchange(outgoing)
    answers = expert(arrived, [g, u, d, *from_left, *from_right, *far], capacity)
    returned = exchange(answers)
    return combine(returned, middle, routing, route_weight, experts, capacity)


def solution(mesh):
    n_sp, n_tp = mesh.shape["sp"], mesh.shape["tp"]
    fine = Mesh(mesh.devices.reshape(n_sp // 2, 2, n_tp), ("chip", "core", "tp"))
    sp = ("chip", "core")
    rows = P(("chip", "core", "tp"), None)
    heads = P(sp, "tp")
    placed = (
        rows,
        *([heads] * 8),
        P(),
        P(),
        P(),
        rows,
        rows,
        P(sp, None, "tp"),
        P(sp, None, "tp"),
        P(sp, "tp", None),
    )
    return jax.shard_map(body, mesh=fine, in_specs=placed, out_specs=rows, check_vma=False)
```

time: 533 us -> 365 us (0.68)
  local copies, waits for them, and re-layouts: 127 us -> 11.9 us
  blocking collectives: 164 us -> 49.2 us
  starting transfers between devices: 18.5 us -> 58.8 us
  waiting for transfers between devices: 161 us -> 200 us
  Pallas kernels: 0 us -> 26.5 us
  matrix products: 23.7 us -> 0 us
  other arithmetic: 16.4 us -> 4.02 us
  loops' own time: 6.28 us -> 0 us
    all_to_all x1 -> x0, blocking collectives: 116 us -> none  [body(): lax.all_to_all(outgoing, 'sp', split_axis=0, concat_axis=0, tiled=True)]
    dynamic_slice x58 -> x0, local copies, waits for them, and re-layouts: 73.7 us -> none  [the longest x32 51.8 us: take_block(): return lax.dynamic_slice_in_dim(source, inside, block_size, 0)]
    ppermute x0 -> x12, waiting for transfers between devices: none -> 72.2 us  [the longest x3 27.9 us: body(): from_left = [lax.ppermute(w, 'tp', ahead) for w in (g, u, d)]]
    reduce_scatter x1 -> x0, waiting for transfers between devices: 50 us -> none  [body(): lax.psum_scatter(jnp.dot(hidden, down_weight[0], preferred_element_type=j...]
    pallas_call x0 -> x7, Pallas kernels: none -> 26.5 us  [the longest x2 12.1 us: attend_chunk(): pl.pallas_call(functools.partial(attention_kernel, flip=flip, row0=row0,...]
    all_to_all x3, starting transfers between devices: 18.3 us -> 43.5 us  [the longest x2 36.4 us: exchange(): lax.all_to_all(slots, ('chip', 'core'), split_axis=0, concat_axis=0, tile...]
    dot_general x13 -> x0, matrix products: 23.7 us -> none  [the longest x1 9.09 us: body(): jnp.dot(hidden, down_weight[0], preferred_element_type=jnp.float32)]
    all_gather x2, waiting for transfers between devices: 77.8 us -> 98.6 us  [the longest x1 75.3 us: body(): chunk_b = lax.all_gather(got, 'chip', axis=0, tiled=True)]
  transfers between devices with their start and end apart: 6 -> 17, of which waited for: 6 -> 11; matrix products, arithmetic and copies ran while one was open for 6% -> 1% of each run, Pallas kernels for 0% -> 3%
where the time goes in v1:
time: 365 us; the launch traced here: 364 us
  waiting for transfers between devices  200 us (55%)
  starting transfers between devices  58.8 us (16%)
  blocking collectives  49.2 us (13%)
  Pallas kernels  26.5 us (7%)
  between operations  13.5 us (4%)
  local copies, waits for them, and re-layouts  11.9 us (3%)
  other arithmetic  4.02 us (1%)
    all_gather x1, waiting for transfers between devices, body(): chunk_b = lax.all_gather(got, 'chip', axis=0, tiled=True)  75.3 us
    all_gather x1, blocking collectives, body(): lax.all_gather(running_sums(gate_wide, gate_narrow), ('chip', 'core'), ax...  49.2 us
    all_to_all x2, starting transfers between devices, exchange(): lax.all_to_all(slots, ('chip', 'core'), split_axis=0, concat_axis=0, tile...  36.4 us
    all_to_all x2, waiting for transfers between devices, exchange(): lax.all_to_all(slots, ('chip', 'core'), split_axis=0, concat_axis=0, tile...  28.1 us
    ppermute x3, waiting for transfers between devices, body(): from_left = [lax.ppermute(w, 'tp', ahead) for w in (g, u, d)]  27.9 us
    ppermute x1, waiting for transfers between devices, body(): lax.ppermute(from_left[2][:part], 'tp', ahead)  26.3 us
    all_gather x1, waiting for transfers between devices, body(): chunk_a = lax.all_gather(keep, 'chip', axis=0, tiled=True)  23.3 us
    pallas_call x2, Pallas kernels, attend_chunk(): pl.pallas_call(functools.partial(attention_kernel, flip=flip, row0=row0,...  12.1 us
  transfers between devices with their start and end apart: 17, of which 11 were waited for; matrix products, arithmetic and copies ran while one was open for 1% of the time, Pallas kernels for 3%

profile of v1, /device:TPU:1, one launch (start us, length us, event | category | flops | bytes accessed | tf_op | source)
XLA Modules:
  0.0 364.3 jit_solution(16781680338860977363)
XLA Ops:
  8.3 3.3 collective-permute-start.1
  14.5 1.5 running.1
  16.0 49.2 %all-gather = f32[512,128]{1,0:T(8,128)} all-gather(f32[8,128]{1,0:T(8,128)} %running.1), channel_id=2, replica_groups=mesh['chip'=32,'core'=2,'tp'=4] {'chip','core'}, dimensions={0}, use_global_device_ids=true | all-gather | bytes 266240 | tf_op jit(solution)/shard_map/all_gather | solution.py:417
  65.2 1.8 offset.1.dk_ref
  68.6 23.3 %all-gather.6.cloned.1.call-done.kv_ref = bf16[8192,256]{1,0:T(8,128)(2,1)} async-done(((bf16[256,256]{1,0:T(8,128)(2,1)}), bf16[8192,256]{1,0:T(8,128)(2,1)}) %all-gather.6.cloned.1.call-update) | async-done | bytes 4194320 | tf_op jit(solution)/shard_map/all_gather | solution.py:414
  91.9 5.9 %attend.2 = (f32[2,512,128]{2,1,0:T(8,128)}, f32[2,512,128]{2,1,0:T(8,128)}, f32[2,512,128]{2,1,0:T(8,128)}) custom-call(s32[1]{0:T(128)} %bitcast.place_ref, bf16[512,128]{1,0:T(8,128)(2,1)} %pad_maximum_fusion.q_ref, f32[64,8,128]{2,1,0:T(8,128)} %offset.1.dk_ref, bf16[8192,256]{1,0:T(8,128)(2,1)} %all-gather.6.cloned.1.call-done.kv_ref), custom_call_target="tpu_custom_call" | custom-call | flops 4294967296 | bytes 4194304 | tf_op jit(solution)/shard_map/attend/pallas_call | solution.py:141
  97.8 75.3 %all-gather.4.cloned.1.call-done.kv_ref = bf16[8192,256]{1,0:T(8,128)(2,1)} async-done(((bf16[256,256]{1,0:T(8,128)(2,1)}), bf16[8192,256]{1,0:T(8,128)(2,1)}) %all-gather.4.cloned.1.call-update) | async-done | bytes 4194320 | tf_op jit(solution)/shard_map/all_gather | solution.py:415
  173.1 6.2 %attend.3 = bf16[512,128]{1,0:T(8,128)(2,1)} custom-call(s32[1]{0:T(128)} %bitcast.place_ref, bf16[512,128]{1,0:T(8,128)(2,1)} %pad_maximum_fusion.q_ref, f32[64,8,128]{2,1,0:T(8,128)} %offset.1.dk_ref, bf16[8192,256]{1,0:T(8,128)(2,1)} %all-gather.4.cloned.1.call-done.kv_ref, f32[2,512,128]{2,1,0:T(8,128)} %get-tuple-element.10.rest_0_, ...), custom_call_target="tpu_custom_call" | custom-call | flops 4294967296 | bytes 4194304 | tf_op jit(solution)/shard_map/attend/pallas_call | solution.py:141
  179.3 7.1 %all-to-all-start = ((bf16[8,64,128]{2,1,0:T(8,128)(2,1)}), bf16[8,64,128]{2,1,0:T(8,128)(2,1)S(1)}, u32[]{:S(2)}, u32[]{:S(2)}) async-start(bf16[8,64,128]{2,1,0:T(8,128)(2,1)} %bitcast.27), calls=%async_computation | async-start | bytes 262144 | tf_op jit(solution)/shard_map/all_to_all | solution.py:423
  186.3 1.4 collective-permute-start.4
  187.7 1.2 collective-permute-start.2
  188.9 1.5 collective-permute-start.6
  190.5 1.4 all-to-all-done.att_ref
  191.9 1.6 copy-done.1
  194.4 1.8 project.1
  197.9 21.3 %all-to-all-start.1 = ((bf16[64,8,1024]{2,1,0:T(8,128)(2,1)}), bf16[64,8,1024]{2,1,0:T(8,128)(2,1)S(1)}, u32[]{:S(2)}, u32[]{:S(2)}) async-start(bf16[64,8,1024]{2,1,0:T(8,128)(2,1)} %bitcast.21), calls=%async_computation.1 | async-start | bytes 2097152 | tf_op jit(solution)/shard_map/all_to_all | solution.py:435
  219.2 1.3 collective-permute-start.7
  220.7 2.4 collective-permute-start.5
  223.1 13.3 %collective-permute-done.2.rest_3_ = bf16[2048,256]{1,0:T(8,128)(2,1)} collective-permute-done((bf16[2048,256]{1,0:T(8,128)(2,1)S(1)}, bf16[2048,256]{1,0:T(8,128)(2,1)}, u32[]{:S(2)}, u32[]{:S(2)}) %collective-permute-start.2) | collective-permute-done | bytes 1048608 | tf_op jit(solution)/shard_map/ppermute | solution.py:404
  236.4 2.7 collective-permute-start.9
  239.1 1.1 slice.8
  240.2 3.5 collective-permute-done.7.rest_8_
  244.2 14.6 %collective-permute-done.3.rest_4_ = bf16[2048,256]{1,0:T(8,128)(2,1)S(1)} collective-permute-done((bf16[2048,256]{1,0:T(8,128)(2,1)}, bf16[2048,256]{1,0:T(8,128)(2,1)S(1)}, u32[]{:S(2)}, u32[]{:S(2)}) %collective-permute-start.3) | collective-permute-done | bytes 1048608 | tf_op jit(solution)/shard_map/ppermute | solution.py:404
  259.2 6.9 %collective-permute-done.5.rest_6_ = bf16[2048,256]{1,0:T(8,128)(2,1)S(1)} collective-permute-done((bf16[2048,256]{1,0:T(8,128)(2,1)S(1)}, bf16[2048,256]{1,0:T(8,128)(2,1)S(1)}, u32[]{:S(2)}, u32[]{:S(2)}) %collective-permute-start.5) | collective-permute-done | bytes 1048608 | tf_op jit(solution)/shard_map/ppermute | solution.py:405
  266.2 26.3 %collective-permute-done.10.rest_11_ = bf16[128,2048]{1,0:T(8,128)(2,1)S(1)} collective-permute-done((bf16[128,2048]{1,0:T(8,128)(2,1)S(1)}, bf16[128,2048]{1,0:T(8,128)(2,1)S(1)}, u32[]{:S(2)}, u32[]{:S(2)}) %collective-permute-start.10) | collective-permute-done | bytes 524320 | tf_op jit(solution)/shard_map/ppermute | solution.py:410
  293.3 6.6 %collective-permute-done.11.rest_12_ = bf16[128,2048]{1,0:T(8,128)(2,1)S(1)} collective-permute-done((bf16[128,2048]{1,0:T(8,128)(2,1)S(1)}, bf16[128,2048]{1,0:T(8,128)(2,1)S(1)}, u32[]{:S(2)}, u32[]{:S(2)}) %collective-permute-start.11) | collective-permute-done | bytes 524320 | tf_op jit(solution)/shard_map/ppermute | solution.py:411
  300.7 1.0 copy-done.16
  302.8 1.0 copy-done.8
  303.8 7.4 %expert.1 = bf16[512,1024]{1,0:T(8,128)(2,1)} custom-call(bf16[512,1024]{1,0:T(8,128)(2,1)S(1)} %bitcast.13, bf16[2048,256]{1,0:T(8,128)(2,1)S(1)} %bitcast.17, bf16[2048,256]{1,0:T(8,128)(2,1)S(1)} %bitcast.20, bf16[256,2048]{1,0:T(8,128)(2,1)} %bitcast.25, bf16[2048,256]{1,0:T(8,128)(2,1)} %collective-permute-done.2.rest_3_, bf16[2048,256]{1,0:T(8,128)(2,1)} %copy-done.14, ...), custom_call_target="tpu_custom_call" | custom-call | flops 3221225472 | bytes 12582912 | tf_op jit(solution)/shard_map/expert/pallas_call | solution.py:324
  311.3 15.1 %all-to-all-start.2 = ((bf16[64,8,1024]{2,1,0:T(8,128)(2,1)}), bf16[64,8,1024]{2,1,0:T(8,128)(2,1)S(1)}, u32[]{:S(2)}, u32[]{:S(2)}) async-start(bf16[64,8,1024]{2,1,0:T(8,128)(2,1)} %bitcast.11), calls=%async_computation.2 | async-start | bytes 2097152 | tf_op jit(solution)/shard_map/all_to_all | solution.py:435
  326.5 28.1 %all-to-all-done.2 = bf16[64,8,1024]{2,1,0:T(8,128)(2,1)S(1)} async-done(((bf16[64,8,1024]{2,1,0:T(8,128)(2,1)}), bf16[64,8,1024]{2,1,0:T(8,128)(2,1)S(1)}, u32[]{:S(2)}, u32[]{:S(2)}) %all-to-all-start.2) | async-done | bytes 1048608 | tf_op jit(solution)/shard_map/all_to_all | solution.py:435
  355.5 1.9 combine.1
  (62 shorter events, 13.8 us)
Async XLA Ops:
  6.5 85.4 %all-gather.6.cloned.1.call-start = ((), (), s32[]{:S(2)}) async-start(), calls=%async_computation.4 | async-start | bytes 4325376 | tf_op jit(solution)/shard_map/all_gather | solution.py:414
  8.2 164.9 %all-gather.4.cloned.1.call-start = ((), (), s32[]{:S(2)}) async-start(), calls=%async_computation.3 | async-start | bytes 4325376 | tf_op jit(solution)/shard_map/all_gather | solution.py:415
  8.3 4.3 %collective-permute-start.1 = (bf16[256,256]{1,0:T(8,128)(2,1)S(1)}, bf16[256,256]{1,0:T(8,128)(2,1)S(1)}, u32[]{:S(2)}, u32[]{:S(2)}) collective-permute-start(bf16[256,256]{1,0:T(8,128)(2,1)S(1)} %pad_maximum_fusion.1), channel_id=1, source_target_pairs={{0,4},{4,0},{1,5},{5,1},{2,6},{6,2},{3,7},{7,3},{8,12},{12,8},{9,1... | collective-permute-start | bytes 393224 | tf_op jit(solution)/shard_map/ppermute | solution.py:396
  14.1 53.0 %collective-permute-start = (bf16[256,128]{1,0:T(8,128)(2,1)S(1)}, bf16[256,128]{1,0:T(8,128)(2,1)S(1)}, u32[]{:S(2)}, u32[]{:S(2)}) collective-permute-start(bf16[256,128]{1,0:T(8,128)(2,1)S(1)} %broadcast_select_fusion.6), channel_id=1, source_target_pairs={{0,4},{4,0},{1,5},{5,1},{2,6},{6,2},{3,7},{7,3},{8,12},{12,8},{9,1... | collective-permute-start | bytes 196616 | tf_op jit(solution)/shard_map/ppermute | solution.py:398
  173.1 14.6 %copy-start.2 = (bf16[1,2048,256]{2,1,0:T(8,128)(2,1)S(1)}, bf16[1,2048,256]{2,1,0:T(8,128)(2,1)}, u32[]{:S(2)}) copy-start(bf16[1,2048,256]{2,1,0:T(8,128)(2,1)} %param.31) | copy-start | bytes 3145732
  173.1 17.3 %copy-start.18 = (s32[64,2]{0,1:T(2,128)S(1)}, s32[64,2]{0,1:T(2,128)}, u32[]{:S(2)}) copy-start(s32[64,2]{0,1:T(2,128)} %param.29) | copy-start | bytes 1540
  173.1 18.8 %copy-start = (bf16[512,2048]{1,0:T(8,128)(2,1)S(1)}, bf16[512,2048]{1,0:T(8,128)(2,1)}, u32[]{:S(2)}) copy-start(bf16[512,2048]{1,0:T(8,128)(2,1)} %wide_ref.1) | copy-start | bytes 6291460
  173.1 18.8 %copy-start.12 = (f32[2048]{0:T(1024)S(1)}, f32[2048]{0:T(1024)}, u32[]{:S(2)}) copy-start(f32[2048]{0:T(1024)} %param.28) | copy-start | bytes 24580
  179.3 12.6 %all-to-all-start = ((bf16[8,64,128]{2,1,0:T(8,128)(2,1)}), bf16[8,64,128]{2,1,0:T(8,128)(2,1)S(1)}, u32[]{:S(2)}, u32[]{:S(2)}) async-start(bf16[8,64,128]{2,1,0:T(8,128)(2,1)} %bitcast.27), calls=%async_computation | async-start | bytes 262144 | tf_op jit(solution)/shard_map/all_to_all | solution.py:423
  186.3 34.4 %collective-permute-start.4 = (bf16[256,2048]{1,0:T(8,128)(2,1)}, bf16[256,2048]{1,0:T(8,128)(2,1)}, u32[]{:S(2)}, u32[]{:S(2)}) collective-permute-start(bf16[256,2048]{1,0:T(8,128)(2,1)} %bitcast.23), channel_id=1, source_target_pairs={{0,1},{1,2},{2,3},{3,0},{4,5},{5,6},{6,7},{7,4},{8,9},{9,10},{10,1... | collective-permute-start | bytes 3145736 | tf_op jit(solution)/shard_map/ppermute | solution.py:404
  187.7 48.7 %collective-permute-start.2 = (bf16[2048,256]{1,0:T(8,128)(2,1)S(1)}, bf16[2048,256]{1,0:T(8,128)(2,1)}, u32[]{:S(2)}, u32[]{:S(2)}) collective-permute-start(bf16[2048,256]{1,0:T(8,128)(2,1)S(1)} %bitcast.15), channel_id=1, source_target_pairs={{0,1},{1,2},{2,3},{3,0},{4,5},{5,6},{6,7},{7,4},{8,9},{9,10},{10,1... | collective-permute-start | bytes 3145736 | tf_op jit(solution)/shard_map/ppermute | solution.py:404
  188.9 47.5 %collective-permute-start.6 = (bf16[2048,256]{1,0:T(8,128)(2,1)}, bf16[2048,256]{1,0:T(8,128)(2,1)}, u32[]{:S(2)}, u32[]{:S(2)}) collective-permute-start(bf16[2048,256]{1,0:T(8,128)(2,1)} %bitcast.18), channel_id=1, source_target_pairs={{0,3},{1,0},{2,1},{3,2},{4,7},{5,4},{6,5},{7,6},{8,11},{9,8},{10,9... | collective-permute-start | bytes 3145736 | tf_op jit(solution)/shard_map/ppermute | solution.py:405
  191.9 1.6 copy-start.1
  196.2 1.0 copy-start.4
  197.9 103.9 %copy-start.3 = (bf16[1,2048,256]{2,1,0:T(8,128)(2,1)S(1)}, bf16[1,2048,256]{2,1,0:T(8,128)(2,1)}, u32[]{:S(2)}) copy-start(bf16[1,2048,256]{2,1,0:T(8,128)(2,1)} %param.32) | copy-start | bytes 3145732
  197.9 103.9 %all-to-all-start.1 = ((bf16[64,8,1024]{2,1,0:T(8,128)(2,1)}), bf16[64,8,1024]{2,1,0:T(8,128)(2,1)S(1)}, u32[]{:S(2)}, u32[]{:S(2)}) async-start(bf16[64,8,1024]{2,1,0:T(8,128)(2,1)} %bitcast.21), calls=%async_computation.1 | async-start | bytes 2097152 | tf_op jit(solution)/shard_map/all_to_all | solution.py:435
  219.2 24.6 %collective-permute-start.7 = (bf16[256,2048]{1,0:T(8,128)(2,1)}, bf16[256,2048]{1,0:T(8,128)(2,1)S(1)}, u32[]{:S(2)}, u32[]{:S(2)}) collective-permute-start(bf16[256,2048]{1,0:T(8,128)(2,1)} %bitcast.24), channel_id=1, source_target_pairs={{0,3},{1,0},{2,1},{3,2},{4,7},{5,4},{6,5},{7,6},{8,11},{9,8},{10,9... | collective-permute-start | bytes 3145736 | tf_op jit(solution)/shard_map/ppermute | solution.py:405
  220.4 38.3 %collective-permute-start.3 = (bf16[2048,256]{1,0:T(8,128)(2,1)}, bf16[2048,256]{1,0:T(8,128)(2,1)S(1)}, u32[]{:S(2)}, u32[]{:S(2)}) collective-permute-start(bf16[2048,256]{1,0:T(8,128)(2,1)} %bitcast.19), channel_id=1, source_target_pairs={{0,1},{1,2},{2,3},{3,0},{4,5},{5,6},{6,7},{7,4},{8,9},{9,10},{10,1... | collective-permute-start | bytes 3145736 | tf_op jit(solution)/shard_map/ppermute | solution.py:404
  220.7 45.5 %collective-permute-start.5 = (bf16[2048,256]{1,0:T(8,128)(2,1)S(1)}, bf16[2048,256]{1,0:T(8,128)(2,1)S(1)}, u32[]{:S(2)}, u32[]{:S(2)}) collective-permute-start(bf16[2048,256]{1,0:T(8,128)(2,1)S(1)} %bitcast.16), channel_id=1, source_target_pairs={{0,3},{1,0},{2,1},{3,2},{4,7},{5,4},{6,5},{7,6},{8,11},{9,8},{10,9... | collective-permute-start | bytes 3145736 | tf_op jit(solution)/shard_map/ppermute | solution.py:405
  236.4 64.3 %collective-permute-start.8 = (bf16[2048,256]{1,0:T(8,128)(2,1)}, bf16[2048,256]{1,0:T(8,128)(2,1)S(1)}, u32[]{:S(2)}, u32[]{:S(2)}) collective-permute-start(bf16[2048,256]{1,0:T(8,128)(2,1)} %collective-permute-done.2.rest_3_), channel_id=1, source_target_pairs={{0,1},{1,2},{2,3},{3,0},{4,5},{5,6},{6,7},{7,4},{8,9},{9,10},{10,1... | collective-permute-start | bytes 3145736 | tf_op jit(solution)/shard_map/ppermute | solution.py:408
  236.4 65.3 %collective-permute-start.9 = (bf16[2048,256]{1,0:T(8,128)(2,1)}, bf16[2048,256]{1,0:T(8,128)(2,1)}, u32[]{:S(2)}, u32[]{:S(2)}) collective-permute-start(bf16[2048,256]{1,0:T(8,128)(2,1)} %collective-permute-done.6.rest_7_), channel_id=1, source_target_pairs={{0,3},{1,0},{2,1},{3,2},{4,7},{5,4},{6,5},{7,6},{8,11},{9,8},{10,9... | collective-permute-start | bytes 3145736 | tf_op jit(solution)/shard_map/ppermute | solution.py:409
  243.7 57.0 %copy-start.13 = (bf16[256,2048]{1,0:T(8,128)(2,1)}, bf16[256,2048]{1,0:T(8,128)(2,1)S(1)}, u32[]{:S(2)}) copy-start(bf16[256,2048]{1,0:T(8,128)(2,1)S(1)} %collective-permute-done.7.rest_8_) | copy-start | bytes 3145732
  243.7 48.8 %collective-permute-start.10 = (bf16[128,2048]{1,0:T(8,128)(2,1)S(1)}, bf16[128,2048]{1,0:T(8,128)(2,1)S(1)}, u32[]{:S(2)}, u32[]{:S(2)}) collective-permute-start(bf16[128,2048]{1,0:T(8,128)(2,1)S(1)} %slice.8), channel_id=1, source_target_pairs={{0,1},{1,2},{2,3},{3,0},{4,5},{5,6},{6,7},{7,4},{8,9},{9,10},{10,1... | collective-permute-start | bytes 1572872 | tf_op jit(solution)/shard_map/ppermute | solution.py:410
  258.8 41.9 %copy-start.14 = (bf16[2048,256]{1,0:T(8,128)(2,1)}, bf16[2048,256]{1,0:T(8,128)(2,1)S(1)}, u32[]{:S(2)}) copy-start(bf16[2048,256]{1,0:T(8,128)(2,1)S(1)} %collective-permute-done.3.rest_4_) | copy-start | bytes 3145732
  258.8 41.1 %collective-permute-start.11 = (bf16[128,2048]{1,0:T(8,128)(2,1)S(1)}, bf16[128,2048]{1,0:T(8,128)(2,1)S(1)}, u32[]{:S(2)}, u32[]{:S(2)}) collective-permute-start(bf16[128,2048]{1,0:T(8,128)(2,1)S(1)} %slice.9), channel_id=1, source_target_pairs={{0,3},{1,0},{2,1},{3,2},{4,7},{5,4},{6,5},{7,6},{8,11},{9,8},{10,9... | collective-permute-start | bytes 1572872 | tf_op jit(solution)/shard_map/ppermute | solution.py:411
  266.2 34.5 %copy-start.15 = (bf16[2048,256]{1,0:T(8,128)(2,1)}, bf16[2048,256]{1,0:T(8,128)(2,1)S(1)}, u32[]{:S(2)}) copy-start(bf16[2048,256]{1,0:T(8,128)(2,1)S(1)} %collective-permute-done.5.rest_6_) | copy-start | bytes 3145732
  300.7 1.0 copy-start.16
  301.8 1.0 copy-start.6
  302.8 1.0 copy-start.8
  303.8 22.6 %copy-start.19 = (f32[64,2]{0,1:T(2,128)S(1)}, f32[64,2]{0,1:T(2,128)}, u32[]{:S(2)}) copy-start(f32[64,2]{0,1:T(2,128)} %param.30) | copy-start | bytes 1540
  311.3 43.3 %all-to-all-start.2 = ((bf16[64,8,1024]{2,1,0:T(8,128)(2,1)}), bf16[64,8,1024]{2,1,0:T(8,128)(2,1)S(1)}, u32[]{:S(2)}, u32[]{:S(2)}) async-start(bf16[64,8,1024]{2,1,0:T(8,128)(2,1)} %bitcast.11), calls=%async_computation.2 | async-start | bytes 2097152 | tf_op jit(solution)/shard_map/all_to_all | solution.py:435
  354.6 1.0 copy-start.11
  (5 other events, 3.9 us)
Sparse Core Ops, SparseCore 0:
  9.9 81.9 all-gather.5
  94.5 78.5 all-gather.3
